TPU v7x, 32 devices: a whole 2x2x4 slice. The times are simulated.
32 devices in a mesh: sp: 8 (over z, core), tp: 4 (over y, x).
Axes of the slice: x: 2, y: 2, z: 4, core: 2. Of those that a mesh axis runs over, the one named last changes fastest.
Arguments:
- prompt: bfloat16 [8, 2048, 2048], P('tp', 'sp'), may hold values from -6 to 6
- input_gain: float32 [2048], replicated, may hold values from 0.1 to 1.9
- key_weight: bfloat16 [1024, 2048], P('tp'), may hold values from -0.125 to 0.125
- value_weight: bfloat16 [1024, 2048], P('tp'), may hold values from -0.125 to 0.125
- key_gain: float32 [64], replicated, may hold values from 0.1 to 1.9
- queries: bfloat16 [8, 2, 1024], P('sp', None, 'tp'), may hold values from -6 to 6
- score_bias: float32 [2, 16], replicated, may hold values from -9 to -2
Outputs:
- keys: bfloat16 [8, 1024, 2048], P('sp', 'tp')
- values: bfloat16 [8, 1024, 2048], P('sp', 'tp')
- first_read: bfloat16 [8, 2, 1024], P('sp', None, 'tp')
All inputs are finite; a program needn't handle non-finite values.
Results may differ from a plain program's by a relative error of at most 0.01.
Values may be sent and summed in bfloat16 or wider, within the bound.
No kernel may reach another device: no remote copies, remote signals or barrier semaphores. Data moves between devices by JAX's collectives and lax.ppermute only.
A program may use at most 64 MiB of HBM per device.

v0:
```python
import functools
import math

import jax
import jax.numpy as jnp
from jax import lax
from jax.experimental import pallas as pl
from jax.experimental.pallas import tpu as pltpu
from jax.sharding import PartitionSpec as P


HEAD = 64
CORES = 2
CHUNKS = 2

epsilon = 1e-06


def project_kernel(place, gain, *refs, tp, seqs, relays):
    weights = refs[: len(relays)]
    own, other = refs[len(relays) : len(relays) + 2]
    outs = refs[len(relays) + 2 : -4]
    weight_buf, row_buf, weight_sems, row_sems = refs[-4:]
    core = place[0]
    columns, width = weight_buf.shape[1:]
    copies = [
        pltpu.make_async_copy(own, row_buf.at[0], row_sems.at[0]),
        pltpu.make_async_copy(other, row_buf.at[1], row_sems.at[1]),
    ]
    loads = [
        pltpu.make_async_copy(
            ref, weight_buf.at[block, pl.ds(start, size)], weight_sems.at[n]
        )
        for n, (ref, (block, start, size)) in enumerate(zip(weights, relays))
    ]
    for copy in loads + copies:
        copy.start()
    for copy in loads:
        copy.wait()
    stacked = weight_buf[...].reshape(tp * columns, width)
    is_key = core == 0
    for half in range(CORES):
        copies[half].wait()
        for seq in range(seqs):
            raw = lax.dot_general(
                stacked,
                row_buf[half, seq],
                (((1,), (1,)), ((), ())),
                preferred_element_type=jnp.float32,
            )
            heads = raw.reshape(tp * columns // HEAD, HEAD, raw.shape[1])
            scale = lax.rsqrt(jnp.mean(heads * heads, axis=1, keepdims=True) + epsilon)
            factor = jnp.where(is_key, scale * gain[...][None], 1.0)
            done = (heads * factor).reshape(tp, columns, raw.shape[1]).astype(jnp.bfloat16)
            for hop in range(tp):
                outs[hop][seq, (core + half) % CORES] = done[hop]


def project(weights, relays, own, other, place, gain, tp):
    seqs, rows, width = own.shape
    columns = max(start + size for _, start, size in relays)
    anywhere = pl.BlockSpec(memory_space=pl.ANY)
    return pl.pallas_call(
        functools.partial(project_kernel, tp=tp, seqs=seqs, relays=relays),
        out_shape=[jax.ShapeDtypeStruct((seqs, CORES, columns, rows), jnp.bfloat16)] * tp,
        in_specs=[
            pl.BlockSpec(memory_space=pltpu.SMEM),
            pl.BlockSpec(memory_space=pltpu.VMEM),
        ]
        + [anywhere] * (len(weights) + 2),
        out_specs=[pl.BlockSpec(memory_space=pltpu.VMEM)] * tp,
        scratch_shapes=[
            pltpu.VMEM((tp, columns, width), jnp.bfloat16),
            pltpu.VMEM((CORES, seqs, rows, width), jnp.bfloat16),
            pltpu.SemaphoreType.DMA((len(weights),)),
            pltpu.SemaphoreType.DMA((CORES,)),
        ],
        name="project",
    )(place, gain, *weights, own, other)


def order_kernel(place, *refs):
    blocks, out, sems = refs[:-2], refs[-2], refs[-1]
    copies = [
        pltpu.make_async_copy(block, out.at[place[1 + n]], sems.at[n]) for n, block in enumerate(blocks)
    ]
    for copy in copies:
        copy.start()
    for copy in copies:
        copy.wait()


def order(blocks, place):
    anywhere = pl.BlockSpec(memory_space=pl.ANY)
    return pl.pallas_call(
        order_kernel,
        out_shape=jax.ShapeDtypeStruct((len(blocks),) + blocks[0].shape, blocks[0].dtype),
        in_specs=[pl.BlockSpec(memory_space=pltpu.SMEM)] + [anywhere] * len(blocks),
        out_specs=anywhere,
        scratch_shapes=[pltpu.SemaphoreType.DMA((len(blocks),))],
        name="order",
    )(place, *blocks)


def read_kernel(query, bias, *refs):
    pieces = refs[:-6]
    keys, values, read, buf, sems, out_sems = refs[-6:]
    columns = buf.shape[1]
    rows = pieces[0].shape[3]
    step = columns // len(pieces)
    copies = []
    for chunk, piece in enumerate(pieces):
        for source in range(piece.shape[0]):
            for half in range(CORES):
                start = (source // CORES * CORES + half) * rows
                target = buf.at[
                    source % CORES, chunk * step : (chunk + 1) * step, start : start + rows
                ]
                copies.append(
                    pltpu.make_async_copy(
                        piece.at[source, half], target, sems.at[chunk, source, half]
                    )
                )
    for copy in copies:
        copy.start()
    for copy in copies:
        copy.wait()
    outs = [
        pltpu.make_async_copy(buf.at[0], keys, out_sems.at[0]),
        pltpu.make_async_copy(buf.at[1], values, out_sems.at[1]),
    ]
    for copy in outs:
        copy.start()
    length = buf.shape[2]
    group = query.shape[0]
    heads = columns // HEAD
    lanes = lax.broadcasted_iota(jnp.int32, (heads, columns), 1) // HEAD
    mine = lanes == lax.broadcasted_iota(jnp.int32, (heads, columns), 0)
    spread = jnp.concatenate(
        [jnp.where(mine, query[g : g + 1, :].astype(jnp.float32), 0.0) for g in range(group)], axis=0
    ).astype(jnp.bfloat16)
    scores = lax.dot_general(
        spread, buf[0], (((1,), (0,)), ((), ())), preferred_element_type=jnp.float32
    )
    scores = scores / math.sqrt(HEAD) + bias[...]
    keep = -(jnp.maximum(scores, 0.0) + jnp.log1p(jnp.exp(-jnp.abs(scores))))
    span = 128
    after = (
        lax.broadcasted_iota(jnp.int32, (span, span), 0)
        > lax.broadcasted_iota(jnp.int32, (span, span), 1)
    ).astype(jnp.float32)
    carry = jnp.zeros((group * heads, 1), jnp.float32)
    weights = []
    for n in reversed(range(length // span)):
        part = keep[:, n * span : (n + 1) * span]
        later = lax.dot_general(
            part,
            after,
            (((1,), (0,)), ((), ())),
            precision=lax.Precision.HIGHEST,
            preferred_element_type=jnp.float32,
        )
        total = scores[:, n * span : (n + 1) * span] + part + later + carry
        weights.append(jnp.exp(total).astype(jnp.bfloat16))
        carry = carry + jnp.sum(part, axis=1, keepdims=True)
    mixed = lax.dot_general(
        jnp.concatenate(weights[::-1], axis=1),
        buf[1],
        (((1,), (1,)), ((), ())),
        preferred_element_type=jnp.float32,
    )
    read[...] = jnp.concatenate(
        [
            jnp.sum(
                jnp.where(mine, mixed[g * heads : (g + 1) * heads], 0.0), axis=0, keepdims=True
            )
            for g in range(group)
        ],
        axis=0,
    ).astype(jnp.bfloat16)
    for copy in outs:
        copy.wait()


def read_cache(pieces, query, bias, columns, length):
    cache = jax.ShapeDtypeStruct((columns, length), jnp.bfloat16)
    anywhere = pl.BlockSpec(memory_space=pl.ANY)
    vmem = pl.BlockSpec(memory_space=pltpu.VMEM)
    return pl.pallas_call(
        read_kernel,
        out_shape=[cache, cache, jax.ShapeDtypeStruct(query.shape, jnp.bfloat16)],
        in_specs=[vmem, vmem] + [anywhere] * len(pieces),
        out_specs=[anywhere, anywhere, vmem],
        scratch_shapes=[
            pltpu.VMEM((CORES, columns, length), jnp.bfloat16),
            pltpu.SemaphoreType.DMA((len(pieces), pieces[0].shape[0], CORES)),
            pltpu.SemaphoreType.DMA((CORES,)),
        ],
        name="read_cache",
    )(query, bias, *pieces)


def body(prompt, input_gain, key_weight, value_weight, key_gain, queries, score_bias):
    sp, tp = lax.axis_size("sp"), lax.axis_size("tp")
    seqs = prompt.shape[0]
    assert sp == seqs * tp and seqs == CORES
    place_sp, place_tp = lax.axis_index("sp"), lax.axis_index("tp")
    core = place_sp % CORES
    columns = key_weight.shape[0]
    heads_here = columns // HEAD
    chunks = math.gcd(CHUNKS, heads_here)
    step = columns // chunks
    side = math.isqrt(tp)

    def along_tp(array, hop):
        return lax.ppermute(array, "tp", [(n, n ^ hop) for n in range(tp)])

    weight = jnp.where(core == 0, key_weight, value_weight)
    gathered = []
    for chunk in range(chunks):
        part = weight[chunk * step : (chunk + 1) * step]
        if side == 2:
            half = step // 2
            low, high = part[:half], part[half:]
            if gathered:
                low, high, _ = lax.optimization_barrier((low, high, gathered[-1][0][2:6]))
            near_high = along_tp(high, 1)
            far_low = along_tp(low, side)
            near_low = along_tp(low, 1)
            far_high = along_tp(high, side)
            relayed = along_tp(far_low, 1)
            crossed = along_tp(near_high, side)
            blocks = [low, high, near_low, near_high, far_low, far_high, relayed, crossed]
            gathered.append((blocks, tuple((n // 2, n % 2 * half, half) for n in range(2 * tp))))
        else:
            gathered.append(
                (
                    [part] + [along_tp(part, hop) for hop in range(1, tp)],
                    tuple((hop, 0, step) for hop in range(tp)),
                )
            )

    flat = prompt.astype(jnp.float32)
    normed = (
        flat * lax.rsqrt(jnp.mean(flat * flat, axis=-1, keepdims=True) + epsilon) * input_gain
    ).astype(jnp.bfloat16)
    other = lax.ppermute(normed, "sp", [(n, n ^ 1) for n in range(sp)])

    peers = place_tp ^ jnp.arange(tp, dtype=jnp.int32)
    place = jnp.concatenate([core[None], peers]).astype(jnp.int32)
    pieces = []
    ordered = ()
    for blocks, relays in gathered:
        low, own, _ = lax.optimization_barrier((blocks[0], normed, ordered))
        blocks = [low] + blocks[1:]
        outs = project(blocks, relays, own, other, place, key_gain[:, None], tp)
        ordered = order([outs[0]] + [along_tp(outs[hop], hop) for hop in range(1, tp)], place)
        by_sequence = ordered.reshape((sp,) + ordered.shape[2:])
        pieces.append(lax.all_to_all(by_sequence, "sp", split_axis=0, concat_axis=0, tiled=True))

    heads = lax.dynamic_slice_in_dim(score_bias, place_tp * heads_here, heads_here, 1)
    keys, values, read = read_cache(
        pieces, queries[0], heads.reshape(-1, 1), columns, prompt.shape[1] * sp
    )
    return keys[None], values[None], read[None]


def solution(mesh):
    placed = (P("tp", "sp", None), P(), P("tp", None), P("tp", None), P(), P("sp", None, "tp"), P())
    return jax.shard_map(
        body,
        mesh=mesh,
        in_specs=placed,
        out_specs=(P("sp", "tp", None), P("sp", "tp", None), P("sp", None, "tp")),
        check_vma=False,
    )
```

profile of v0, /device:TPU:0, one launch (start us, length us, event | category | flops | bytes accessed | tf_op | source)
XLA Modules:
  0.0 203.3 jit_solution(4681333718744384267)
XLA Ops:
  0.7 2.2 %fusion = f32[2,256]{1,0:T(2,128)S(1)} fusion(bf16[2,256,2048]{2,1,0:T(8,128)(2,1)} %param.7), kind=kLoop, calls=%fused_computation.2 | loop fusion | flops 3145216 | bytes 2099200 | tf_op jit(solution)/shard_map/reduce_sum | solution.py:245
  2.9 1.3 fusion.2.refs_8_
  4.3 0.6 collective-permute-start.6
  5.1 0.5 copy-done.1
  5.6 3.1 %collective-permute-start.2 = (bf16[64,2048]{1,0:T(8,128)(2,1)S(1)}, bf16[64,2048]{1,0:T(8,128)(2,1)S(1)}, u32[]{:S(2)}, u32[]{:S(2)}) collective-permute-start(bf16[64,2048]{1,0:T(8,128)(2,1)S(1)} %get-tuple-element.20.refs_0_), channel_id=1, source_target_pairs={{0,2},{1,3},{2,0},{3,1},{4,6},{5,7},{6,4},{7,5},{8,10},{9,11},{10,... | collective-permute-start | bytes 786440 | tf_op jit(solution)/shard_map/ppermute | solution.py:216
  8.7 1.5 collective-permute-start.1
  10.2 0.5 collective-permute-start
  10.8 5.0 %collective-permute-done.2.refs_4_ = bf16[64,2048]{1,0:T(8,128)(2,1)S(1)} collective-permute-done((bf16[64,2048]{1,0:T(8,128)(2,1)S(1)}, bf16[64,2048]{1,0:T(8,128)(2,1)S(1)}, u32[]{:S(2)}, u32[]{:S(2)}) %collective-permute-start.2) | collective-permute-done | bytes 262176 | tf_op jit(solution)/shard_map/ppermute | solution.py:216
  15.7 2.1 %collective-permute-start.4 = (bf16[64,2048]{1,0:T(8,128)(2,1)S(1)}, bf16[64,2048]{1,0:T(8,128)(2,1)}, u32[]{:S(2)}, u32[]{:S(2)}) collective-permute-start(bf16[64,2048]{1,0:T(8,128)(2,1)S(1)} %collective-permute-done.2.refs_4_), channel_id=1, source_target_pairs={{0,1},{1,0},{2,3},{3,2},{4,5},{5,4},{6,7},{7,6},{8,9},{9,8},{10,11... | collective-permute-start | bytes 786440 | tf_op jit(solution)/shard_map/ppermute | solution.py:216
  17.9 1.4 collective-permute-start.5
  19.3 0.7 copy.10.gain
  20.1 0.6 pad_add_fusion.place
  20.6 2.9 %collective-permute-done.refs_2_ = bf16[64,2048]{1,0:T(8,128)(2,1)} collective-permute-done((bf16[64,2048]{1,0:T(8,128)(2,1)S(1)}, bf16[64,2048]{1,0:T(8,128)(2,1)}, u32[]{:S(2)}, u32[]{:S(2)}) %collective-permute-start) | collective-permute-done | bytes 262176 | tf_op jit(solution)/shard_map/ppermute | solution.py:216
  23.6 5.1 %collective-permute-done.4.refs_6_ = bf16[64,2048]{1,0:T(8,128)(2,1)} collective-permute-done((bf16[64,2048]{1,0:T(8,128)(2,1)S(1)}, bf16[64,2048]{1,0:T(8,128)(2,1)}, u32[]{:S(2)}, u32[]{:S(2)}) %collective-permute-start.4) | collective-permute-done | bytes 262176 | tf_op jit(solution)/shard_map/ppermute | solution.py:216
  28.7 6.7 %project.2 = (bf16[2,2,128,256]{3,2,1,0:T(8,128)(2,1)}, bf16[2,2,128,256]{3,2,1,0:T(8,128)(2,1)}, bf16[2,2,128,256]{3,2,1,0:T(8,128)(2,1)}, bf16[2,2,128,256]{3,2,1,0:T(8,128)(2,1)}) custom-call(s32[5]{0:T(128)} %pad_add_fusion.place, f32[64,1]{1,0:T(8,128)} %copy.10.gain, bf16[64,2048]{1,0:T(8,128)(2,1)} %copy-done.9, bf16[64,2048]{1,0:T(8,128)(2,1)} %copy-done.8, ...), custom_call_target="tpu_custom_call" | custom-call | tf_op jit(solution)/shard_map/project/pallas_call | solution.py:63
  35.5 1.6 collective-permute-start.7
  37.0 0.5 collective-permute-start.8
  37.5 1.5 collective-permute-start.9
  39.0 5.9 %collective-permute-done.7.refs_1_ = bf16[2,2,128,256]{3,2,1,0:T(8,128)(2,1)S(1)} collective-permute-done((bf16[2,2,128,256]{3,2,1,0:T(8,128)(2,1)}, bf16[2,2,128,256]{3,2,1,0:T(8,128)(2,1)S(1)}, u32[]{:S(2)}, u32[]{:S(2)}) %collective-permute-start.7) | collective-permute-done | bytes 262176 | tf_op jit(solution)/shard_map/ppermute | solution.py:216
  44.9 5.5 %collective-permute-done.8.refs_2_ = bf16[2,2,128,256]{3,2,1,0:T(8,128)(2,1)S(1)} collective-permute-done((bf16[2,2,128,256]{3,2,1,0:T(8,128)(2,1)}, bf16[2,2,128,256]{3,2,1,0:T(8,128)(2,1)S(1)}, u32[]{:S(2)}, u32[]{:S(2)}) %collective-permute-start.8) | collective-permute-done | bytes 262176 | tf_op jit(solution)/shard_map/ppermute | solution.py:216
  50.4 0.7 copy-done.20
  51.2 33.6 %order.2 = bf16[4,2,2,128,256]{4,3,2,1,0:T(8,128)(2,1)} custom-call(s32[5]{0:T(128)} %pad_add_fusion.place, bf16[2,2,128,256]{3,2,1,0:T(8,128)(2,1)} %get-tuple-element.22.refs_0_, bf16[2,2,128,256]{3,2,1,0:T(8,128)(2,1)} %copy-done.18, bf16[2,2,128,256]{3,2,1,0:T(8,128)(2,1)} %copy-done.20, bf16[2,2,128,256]{3,2,1,0:T(8,128)(2,1)} %copy-done.22), custom_call_target="tpu_custom_call" | custom-call | tf_op jit(solution)/shard_map/order/pallas_call | solution.py:95
  84.8 4.9 %all-to-all-start = ((bf16[8,2,128,256]{3,2,1,0:T(8,128)(2,1)}), bf16[8,2,128,256]{3,2,1,0:T(8,128)(2,1)S(1)}, u32[]{:S(2)}, u32[]{:S(2)}) async-start(bf16[8,2,128,256]{3,2,1,0:T(8,128)(2,1)} %bitcast.8), calls=%async_computation | async-start | bytes 2097152 | tf_op jit(solution)/shard_map/all_to_all | solution.py:259
  89.7 0.5 collective-permute-start.12
  90.2 1.1 collective-permute-start.11
  91.3 0.9 collective-permute-start.10
  92.3 1.5 collective-permute-start.13
  93.8 5.1 %collective-permute-done.12.refs_4_ = bf16[64,2048]{1,0:T(8,128)(2,1)S(1)} collective-permute-done((bf16[64,2048]{1,0:T(8,128)(2,1)S(1)}, bf16[64,2048]{1,0:T(8,128)(2,1)S(1)}, u32[]{:S(2)}, u32[]{:S(2)}) %collective-permute-start.12) | collective-permute-done | bytes 262176 | tf_op jit(solution)/shard_map/ppermute | solution.py:216
  98.9 0.5 collective-permute-start.14
  99.4 1.5 collective-permute-start.15
  100.9 4.1 %collective-permute-done.10.refs_2_ = bf16[64,2048]{1,0:T(8,128)(2,1)S(1)} collective-permute-done((bf16[64,2048]{1,0:T(8,128)(2,1)S(1)}, bf16[64,2048]{1,0:T(8,128)(2,1)S(1)}, u32[]{:S(2)}, u32[]{:S(2)}) %collective-permute-start.10) | collective-permute-done | bytes 262176 | tf_op jit(solution)/shard_map/ppermute | solution.py:216
  105.0 4.9 %collective-permute-done.14.refs_6_ = bf16[64,2048]{1,0:T(8,128)(2,1)S(1)} collective-permute-done((bf16[64,2048]{1,0:T(8,128)(2,1)S(1)}, bf16[64,2048]{1,0:T(8,128)(2,1)S(1)}, u32[]{:S(2)}, u32[]{:S(2)}) %collective-permute-start.14) | collective-permute-done | bytes 262176 | tf_op jit(solution)/shard_map/ppermute | solution.py:216
  110.0 0.7 copy-done.15
  110.6 0.7 copy-done.16
  111.3 6.7 %project.3 = (bf16[2,2,128,256]{3,2,1,0:T(8,128)(2,1)}, bf16[2,2,128,256]{3,2,1,0:T(8,128)(2,1)}, bf16[2,2,128,256]{3,2,1,0:T(8,128)(2,1)}, bf16[2,2,128,256]{3,2,1,0:T(8,128)(2,1)}) custom-call(s32[5]{0:T(128)} %pad_add_fusion.place, f32[64,1]{1,0:T(8,128)} %copy.10.gain, bf16[64,2048]{1,0:T(8,128)(2,1)} %copy-done.7, bf16[64,2048]{1,0:T(8,128)(2,1)} %copy-done.6, ...), custom_call_target="tpu_custom_call" | custom-call | tf_op jit(solution)/shard_map/project/pallas_call | solution.py:63
  118.1 1.2 collective-permute-start.16
  119.2 0.9 collective-permute-start.17
  120.1 1.5 collective-permute-start.18
  121.6 5.9 %collective-permute-done.16.refs_1_ = bf16[2,2,128,256]{3,2,1,0:T(8,128)(2,1)S(1)} collective-permute-done((bf16[2,2,128,256]{3,2,1,0:T(8,128)(2,1)}, bf16[2,2,128,256]{3,2,1,0:T(8,128)(2,1)S(1)}, u32[]{:S(2)}, u32[]{:S(2)}) %collective-permute-start.16) | collective-permute-done | bytes 262176 | tf_op jit(solution)/shard_map/ppermute | solution.py:216
  127.5 0.7 collective-permute-done.17.refs_2_
  128.2 4.2 %collective-permute-done.18.refs_3_ = bf16[2,2,128,256]{3,2,1,0:T(8,128)(2,1)S(1)} collective-permute-done((bf16[2,2,128,256]{3,2,1,0:T(8,128)(2,1)}, bf16[2,2,128,256]{3,2,1,0:T(8,128)(2,1)S(1)}, u32[]{:S(2)}, u32[]{:S(2)}) %collective-permute-start.18) | collective-permute-done | bytes 262176 | tf_op jit(solution)/shard_map/ppermute | solution.py:216
  132.5 0.7 copy-done.21
  133.2 33.6 %order.3 = bf16[4,2,2,128,256]{4,3,2,1,0:T(8,128)(2,1)} custom-call(s32[5]{0:T(128)} %pad_add_fusion.place, bf16[2,2,128,256]{3,2,1,0:T(8,128)(2,1)} %get-tuple-element.30.refs_0_, bf16[2,2,128,256]{3,2,1,0:T(8,128)(2,1)} %copy-done.17, bf16[2,2,128,256]{3,2,1,0:T(8,128)(2,1)} %copy-done.19, bf16[2,2,128,256]{3,2,1,0:T(8,128)(2,1)} %copy-done.21), custom_call_target="tpu_custom_call" | custom-call | tf_op jit(solution)/shard_map/order/pallas_call | solution.py:95
  166.8 4.3 %all-to-all-start.1 = ((bf16[8,2,128,256]{3,2,1,0:T(8,128)(2,1)}), bf16[8,2,128,256]{3,2,1,0:T(8,128)(2,1)S(1)}, u32[]{:S(2)}, u32[]{:S(2)}) async-start(bf16[8,2,128,256]{3,2,1,0:T(8,128)(2,1)} %bitcast.9), calls=%async_computation.1 | async-start | bytes 2097152 | tf_op jit(solution)/shard_map/all_to_all | solution.py:259
  171.2 0.7 reshape.27.bias
  171.9 25.8 %all-to-all-done.1.refs_1_ = bf16[8,2,128,256]{3,2,1,0:T(8,128)(2,1)S(1)} async-done(((bf16[8,2,128,256]{3,2,1,0:T(8,128)(2,1)}), bf16[8,2,128,256]{3,2,1,0:T(8,128)(2,1)S(1)}, u32[]{:S(2)}, u32[]{:S(2)}) %all-to-all-start.1) | async-done | bytes 1048608 | tf_op jit(solution)/shard_map/all_to_all | solution.py:259
  197.7 1.0 copy-done.4
  198.7 4.6 %read_cache.1 = (bf16[256,2048]{1,0:T(8,128)(2,1)}, bf16[256,2048]{1,0:T(8,128)(2,1)}, bf16[2,256]{1,0:T(2,128)(2,1)}) custom-call(bf16[2,256]{1,0:T(2,128)(2,1)} %bitcast.10, f32[8,1]{1,0:T(8,128)} %reshape.27.bias, bf16[8,2,128,256]{3,2,1,0:T(8,128)(2,1)} %copy-done.3, bf16[8,2,128,256]{3,2,1,0:T(8,128)(2,1)} %copy-done.4), custom_call_target="tpu_custom_call" | custom-call | tf_op jit(solution)/shard_map/read_cache/pallas_call | solution.py:189
  (57 shorter events, 0.7 us)
Async XLA Ops:
  0.6 170.5 %copy-start = (f32[2,16]{1,0:T(2,128)S(1)}, f32[2,16]{1,0:T(2,128)}, u32[]{:S(2)}) copy-start(f32[2,16]{1,0:T(2,128)} %param.13) | copy-start | bytes 388
  0.6 2.2 %copy-start.2 = (bf16[2,256,2048]{2,1,0:T(8,128)(2,1)S(1)}, bf16[2,256,2048]{2,1,0:T(8,128)(2,1)}, u32[]{:S(2)}) copy-start(bf16[2,256,2048]{2,1,0:T(8,128)(2,1)} %param.7) | copy-start | bytes 6291460
  2.9 1.9 copy-start.5
  4.2 1.3 copy-start.1
  4.3 24.4 %collective-permute-start.6 = (bf16[2,256,2048]{2,1,0:T(8,128)(2,1)S(1)}, bf16[2,256,2048]{2,1,0:T(8,128)(2,1)}, u32[]{:S(2)}, u32[]{:S(2)}) collective-permute-start(bf16[2,256,2048]{2,1,0:T(8,128)(2,1)S(1)} %fusion.2.refs_8_), channel_id=1, source_target_pairs={{0,4},{4,0},{8,12},{12,8},{16,20},{20,16},{24,28},{28,24},{1,5},{5... | collective-permute-start | bytes 6291464 | tf_op jit(solution)/shard_map/ppermute | solution.py:247
  4.8 14.5 %copy-start.23 = (f32[64]{0:T(128)S(1)}, f32[64]{0:T(128)}, u32[]{:S(2)}) copy-start(f32[64]{0:T(128)} %param.11) | copy-start | bytes 772
  5.6 23.1 %copy-start.8 = (bf16[64,2048]{1,0:T(8,128)(2,1)}, bf16[64,2048]{1,0:T(8,128)(2,1)S(1)}, u32[]{:S(2)}) copy-start(bf16[64,2048]{1,0:T(8,128)(2,1)S(1)} %get-tuple-element.39.refs_1_) | copy-start | bytes 786436
  5.6 23.1 %copy-start.9 = (bf16[64,2048]{1,0:T(8,128)(2,1)}, bf16[64,2048]{1,0:T(8,128)(2,1)S(1)}, u32[]{:S(2)}) copy-start(bf16[64,2048]{1,0:T(8,128)(2,1)S(1)} %get-tuple-element.20.refs_0_) | copy-start | bytes 786436
  5.6 85.8 %copy-start.7 = (bf16[64,2048]{1,0:T(8,128)(2,1)}, bf16[64,2048]{1,0:T(8,128)(2,1)S(1)}, u32[]{:S(2)}) copy-start(bf16[64,2048]{1,0:T(8,128)(2,1)S(1)} %get-tuple-element.27.refs_0_) | copy-start | bytes 786436
  5.6 86.7 %copy-start.6 = (bf16[64,2048]{1,0:T(8,128)(2,1)}, bf16[64,2048]{1,0:T(8,128)(2,1)S(1)}, u32[]{:S(2)}) copy-start(bf16[64,2048]{1,0:T(8,128)(2,1)S(1)} %get-tuple-element.28.refs_1_) | copy-start | bytes 786436
  5.6 10.1 %collective-permute-start.2 = (bf16[64,2048]{1,0:T(8,128)(2,1)S(1)}, bf16[64,2048]{1,0:T(8,128)(2,1)S(1)}, u32[]{:S(2)}, u32[]{:S(2)}) collective-permute-start(bf16[64,2048]{1,0:T(8,128)(2,1)S(1)} %get-tuple-element.20.refs_0_), channel_id=1, source_target_pairs={{0,2},{1,3},{2,0},{3,1},{4,6},{5,7},{6,4},{7,5},{8,10},{9,11},{10,... | collective-permute-start | bytes 786440 | tf_op jit(solution)/shard_map/ppermute | solution.py:216
  8.7 9.3 %collective-permute-start.1 = (bf16[64,2048]{1,0:T(8,128)(2,1)S(1)}, bf16[64,2048]{1,0:T(8,128)(2,1)}, u32[]{:S(2)}, u32[]{:S(2)}) collective-permute-start(bf16[64,2048]{1,0:T(8,128)(2,1)S(1)} %get-tuple-element.39.refs_1_), channel_id=1, source_target_pairs={{0,1},{1,0},{2,3},{3,2},{4,5},{5,4},{6,7},{7,6},{8,9},{9,8},{10,11... | collective-permute-start | bytes 786440 | tf_op jit(solution)/shard_map/ppermute | solution.py:216
  10.2 13.4 %collective-permute-start = (bf16[64,2048]{1,0:T(8,128)(2,1)S(1)}, bf16[64,2048]{1,0:T(8,128)(2,1)}, u32[]{:S(2)}, u32[]{:S(2)}) collective-permute-start(bf16[64,2048]{1,0:T(8,128)(2,1)S(1)} %get-tuple-element.20.refs_0_), channel_id=1, source_target_pairs={{0,1},{1,0},{2,3},{3,2},{4,5},{5,4},{6,7},{7,6},{8,9},{9,8},{10,11... | collective-permute-start | bytes 786440 | tf_op jit(solution)/shard_map/ppermute | solution.py:216
  10.7 12.9 %collective-permute-start.3 = (bf16[64,2048]{1,0:T(8,128)(2,1)S(1)}, bf16[64,2048]{1,0:T(8,128)(2,1)}, u32[]{:S(2)}, u32[]{:S(2)}) collective-permute-start(bf16[64,2048]{1,0:T(8,128)(2,1)S(1)} %get-tuple-element.39.refs_1_), channel_id=1, source_target_pairs={{0,2},{1,3},{2,0},{3,1},{4,6},{5,7},{6,4},{7,5},{8,10},{9,11},{10,... | collective-permute-start | bytes 786440 | tf_op jit(solution)/shard_map/ppermute | solution.py:216
  15.7 13.0 %copy-start.10 = (bf16[64,2048]{1,0:T(8,128)(2,1)}, bf16[64,2048]{1,0:T(8,128)(2,1)S(1)}, u32[]{:S(2)}) copy-start(bf16[64,2048]{1,0:T(8,128)(2,1)S(1)} %collective-permute-done.2.refs_4_) | copy-start | bytes 786436
  15.7 13.0 %collective-permute-start.4 = (bf16[64,2048]{1,0:T(8,128)(2,1)S(1)}, bf16[64,2048]{1,0:T(8,128)(2,1)}, u32[]{:S(2)}, u32[]{:S(2)}) collective-permute-start(bf16[64,2048]{1,0:T(8,128)(2,1)S(1)} %collective-permute-done.2.refs_4_), channel_id=1, source_target_pairs={{0,1},{1,0},{2,3},{3,2},{4,5},{5,4},{6,7},{7,6},{8,9},{9,8},{10,11... | collective-permute-start | bytes 786440 | tf_op jit(solution)/shard_map/ppermute | solution.py:216
  17.9 10.8 %collective-permute-start.5 = (bf16[64,2048]{1,0:T(8,128)(2,1)}, bf16[64,2048]{1,0:T(8,128)(2,1)}, u32[]{:S(2)}, u32[]{:S(2)}) collective-permute-start(bf16[64,2048]{1,0:T(8,128)(2,1)} %collective-permute-done.1.refs_3_), channel_id=1, source_target_pairs={{0,2},{1,3},{2,0},{3,1},{4,6},{5,7},{6,4},{7,5},{8,10},{9,11},{10,... | collective-permute-start | bytes 786440 | tf_op jit(solution)/shard_map/ppermute | solution.py:216
  35.5 9.5 %collective-permute-start.7 = (bf16[2,2,128,256]{3,2,1,0:T(8,128)(2,1)}, bf16[2,2,128,256]{3,2,1,0:T(8,128)(2,1)S(1)}, u32[]{:S(2)}, u32[]{:S(2)}) collective-permute-start(bf16[2,2,128,256]{3,2,1,0:T(8,128)(2,1)} %get-tuple-element.23), channel_id=1, source_target_pairs={{0,1},{1,0},{2,3},{3,2},{4,5},{5,4},{6,7},{7,6},{8,9},{9,8},{10,11... | collective-permute-start | bytes 786440 | tf_op jit(solution)/shard_map/ppermute | solution.py:216
  37.0 13.4 %collective-permute-start.8 = (bf16[2,2,128,256]{3,2,1,0:T(8,128)(2,1)}, bf16[2,2,128,256]{3,2,1,0:T(8,128)(2,1)S(1)}, u32[]{:S(2)}, u32[]{:S(2)}) collective-permute-start(bf16[2,2,128,256]{3,2,1,0:T(8,128)(2,1)} %get-tuple-element.24), channel_id=1, source_target_pairs={{0,2},{1,3},{2,0},{3,1},{4,6},{5,7},{6,4},{7,5},{8,10},{9,11},{10,... | collective-permute-start | bytes 786440 | tf_op jit(solution)/shard_map/ppermute | solution.py:216
  37.5 12.9 %collective-permute-start.9 = (bf16[2,2,128,256]{3,2,1,0:T(8,128)(2,1)}, bf16[2,2,128,256]{3,2,1,0:T(8,128)(2,1)S(1)}, u32[]{:S(2)}, u32[]{:S(2)}) collective-permute-start(bf16[2,2,128,256]{3,2,1,0:T(8,128)(2,1)} %get-tuple-element.25), channel_id=1, source_target_pairs={{0,3},{1,2},{2,1},{3,0},{4,7},{5,6},{6,5},{7,4},{8,11},{9,10},{10,... | collective-permute-start | bytes 786440 | tf_op jit(solution)/shard_map/ppermute | solution.py:216
  44.9 5.5 %copy-start.18 = (bf16[2,2,128,256]{3,2,1,0:T(8,128)(2,1)}, bf16[2,2,128,256]{3,2,1,0:T(8,128)(2,1)S(1)}, u32[]{:S(2)}) copy-start(bf16[2,2,128,256]{3,2,1,0:T(8,128)(2,1)S(1)} %collective-permute-done.7.refs_1_) | copy-start | bytes 786436
  50.4 0.7 copy-start.20
  50.4 0.8 copy-start.22
  84.8 81.9 %all-to-all-start = ((bf16[8,2,128,256]{3,2,1,0:T(8,128)(2,1)}), bf16[8,2,128,256]{3,2,1,0:T(8,128)(2,1)S(1)}, u32[]{:S(2)}, u32[]{:S(2)}) async-start(bf16[8,2,128,256]{3,2,1,0:T(8,128)(2,1)} %bitcast.8), calls=%async_computation | async-start | bytes 2097152 | tf_op jit(solution)/shard_map/all_to_all | solution.py:259
  89.7 9.2 %collective-permute-start.12 = (bf16[64,2048]{1,0:T(8,128)(2,1)S(1)}, bf16[64,2048]{1,0:T(8,128)(2,1)S(1)}, u32[]{:S(2)}, u32[]{:S(2)}) collective-permute-start(bf16[64,2048]{1,0:T(8,128)(2,1)S(1)} %get-tuple-element.27.refs_0_), channel_id=1, source_target_pairs={{0,2},{1,3},{2,0},{3,1},{4,6},{5,7},{6,4},{7,5},{8,10},{9,11},{10,... | collective-permute-start | bytes 786440 | tf_op jit(solution)/shard_map/ppermute | solution.py:216
  90.2 9.2 %collective-permute-start.11 = (bf16[64,2048]{1,0:T(8,128)(2,1)S(1)}, bf16[64,2048]{1,0:T(8,128)(2,1)S(1)}, u32[]{:S(2)}, u32[]{:S(2)}) collective-permute-start(bf16[64,2048]{1,0:T(8,128)(2,1)S(1)} %get-tuple-element.28.refs_1_), channel_id=1, source_target_pairs={{0,1},{1,0},{2,3},{3,2},{4,5},{5,4},{6,7},{7,6},{8,9},{9,8},{10,11... | collective-permute-start | bytes 786440 | tf_op jit(solution)/shard_map/ppermute | solution.py:216
  91.3 13.7 %collective-permute-start.10 = (bf16[64,2048]{1,0:T(8,128)(2,1)S(1)}, bf16[64,2048]{1,0:T(8,128)(2,1)S(1)}, u32[]{:S(2)}, u32[]{:S(2)}) collective-permute-start(bf16[64,2048]{1,0:T(8,128)(2,1)S(1)} %get-tuple-element.27.refs_0_), channel_id=1, source_target_pairs={{0,1},{1,0},{2,3},{3,2},{4,5},{5,4},{6,7},{7,6},{8,9},{9,8},{10,11... | collective-permute-start | bytes 786440 | tf_op jit(solution)/shard_map/ppermute | solution.py:216
  92.3 12.8 %collective-permute-start.13 = (bf16[64,2048]{1,0:T(8,128)(2,1)S(1)}, bf16[64,2048]{1,0:T(8,128)(2,1)S(1)}, u32[]{:S(2)}, u32[]{:S(2)}) collective-permute-start(bf16[64,2048]{1,0:T(8,128)(2,1)S(1)} %get-tuple-element.28.refs_1_), channel_id=1, source_target_pairs={{0,2},{1,3},{2,0},{3,1},{4,6},{5,7},{6,4},{7,5},{8,10},{9,11},{10,... | collective-permute-start | bytes 786440 | tf_op jit(solution)/shard_map/ppermute | solution.py:216
  98.9 11.0 %copy-start.11 = (bf16[64,2048]{1,0:T(8,128)(2,1)}, bf16[64,2048]{1,0:T(8,128)(2,1)S(1)}, u32[]{:S(2)}) copy-start(bf16[64,2048]{1,0:T(8,128)(2,1)S(1)} %collective-permute-done.12.refs_4_) | copy-start | bytes 786436
  98.9 11.0 %collective-permute-start.14 = (bf16[64,2048]{1,0:T(8,128)(2,1)S(1)}, bf16[64,2048]{1,0:T(8,128)(2,1)S(1)}, u32[]{:S(2)}, u32[]{:S(2)}) collective-permute-start(bf16[64,2048]{1,0:T(8,128)(2,1)S(1)} %collective-permute-done.12.refs_4_), channel_id=1, source_target_pairs={{0,1},{1,0},{2,3},{3,2},{4,5},{5,4},{6,7},{7,6},{8,9},{9,8},{10,11... | collective-permute-start | bytes 786440 | tf_op jit(solution)/shard_map/ppermute | solution.py:216
  99.4 10.5 %copy-start.12 = (bf16[64,2048]{1,0:T(8,128)(2,1)}, bf16[64,2048]{1,0:T(8,128)(2,1)S(1)}, u32[]{:S(2)}) copy-start(bf16[64,2048]{1,0:T(8,128)(2,1)S(1)} %collective-permute-done.11.refs_3_) | copy-start | bytes 786436
  99.4 10.5 %collective-permute-start.15 = (bf16[64,2048]{1,0:T(8,128)(2,1)S(1)}, bf16[64,2048]{1,0:T(8,128)(2,1)S(1)}, u32[]{:S(2)}, u32[]{:S(2)}) collective-permute-start(bf16[64,2048]{1,0:T(8,128)(2,1)S(1)} %collective-permute-done.11.refs_3_), channel_id=1, source_target_pairs={{0,2},{1,3},{2,0},{3,1},{4,6},{5,7},{6,4},{7,5},{8,10},{9,11},{10,... | collective-permute-start | bytes 786440 | tf_op jit(solution)/shard_map/ppermute | solution.py:216
  105.0 4.9 %copy-start.13 = (bf16[64,2048]{1,0:T(8,128)(2,1)}, bf16[64,2048]{1,0:T(8,128)(2,1)S(1)}, u32[]{:S(2)}) copy-start(bf16[64,2048]{1,0:T(8,128)(2,1)S(1)} %collective-permute-done.10.refs_2_) | copy-start | bytes 786436
  105.0 4.9 %copy-start.14 = (bf16[64,2048]{1,0:T(8,128)(2,1)}, bf16[64,2048]{1,0:T(8,128)(2,1)S(1)}, u32[]{:S(2)}) copy-start(bf16[64,2048]{1,0:T(8,128)(2,1)S(1)} %collective-permute-done.13.refs_5_) | copy-start | bytes 786436
  109.9 0.7 copy-start.15
  110.6 0.7 copy-start.16
  118.1 9.5 %collective-permute-start.16 = (bf16[2,2,128,256]{3,2,1,0:T(8,128)(2,1)}, bf16[2,2,128,256]{3,2,1,0:T(8,128)(2,1)S(1)}, u32[]{:S(2)}, u32[]{:S(2)}) collective-permute-start(bf16[2,2,128,256]{3,2,1,0:T(8,128)(2,1)} %get-tuple-element.31), channel_id=1, source_target_pairs={{0,1},{1,0},{2,3},{3,2},{4,5},{5,4},{6,7},{7,6},{8,9},{9,8},{10,11... | collective-permute-start | bytes 786440 | tf_op jit(solution)/shard_map/ppermute | solution.py:216
  119.2 9.0 %collective-permute-start.17 = (bf16[2,2,128,256]{3,2,1,0:T(8,128)(2,1)}, bf16[2,2,128,256]{3,2,1,0:T(8,128)(2,1)S(1)}, u32[]{:S(2)}, u32[]{:S(2)}) collective-permute-start(bf16[2,2,128,256]{3,2,1,0:T(8,128)(2,1)} %get-tuple-element.32), channel_id=1, source_target_pairs={{0,2},{1,3},{2,0},{3,1},{4,6},{5,7},{6,4},{7,5},{8,10},{9,11},{10,... | collective-permute-start | bytes 786440 | tf_op jit(solution)/shard_map/ppermute | solution.py:216
  120.1 12.3 %collective-permute-start.18 = (bf16[2,2,128,256]{3,2,1,0:T(8,128)(2,1)}, bf16[2,2,128,256]{3,2,1,0:T(8,128)(2,1)S(1)}, u32[]{:S(2)}, u32[]{:S(2)}) collective-permute-start(bf16[2,2,128,256]{3,2,1,0:T(8,128)(2,1)} %get-tuple-element.33), channel_id=1, source_target_pairs={{0,3},{1,2},{2,1},{3,0},{4,7},{5,6},{6,5},{7,4},{8,11},{9,10},{10,... | collective-permute-start | bytes 786440 | tf_op jit(solution)/shard_map/ppermute | solution.py:216
  127.5 4.9 %copy-start.17 = (bf16[2,2,128,256]{3,2,1,0:T(8,128)(2,1)}, bf16[2,2,128,256]{3,2,1,0:T(8,128)(2,1)S(1)}, u32[]{:S(2)}) copy-start(bf16[2,2,128,256]{3,2,1,0:T(8,128)(2,1)S(1)} %collective-permute-done.16.refs_1_) | copy-start | bytes 786436
  128.2 4.2 %copy-start.19 = (bf16[2,2,128,256]{3,2,1,0:T(8,128)(2,1)}, bf16[2,2,128,256]{3,2,1,0:T(8,128)(2,1)S(1)}, u32[]{:S(2)}) copy-start(bf16[2,2,128,256]{3,2,1,0:T(8,128)(2,1)S(1)} %collective-permute-done.17.refs_2_) | copy-start | bytes 786436
  132.5 0.7 copy-start.21
  166.8 30.9 %copy-start.3 = (bf16[8,2,128,256]{3,2,1,0:T(8,128)(2,1)}, bf16[8,2,128,256]{3,2,1,0:T(8,128)(2,1)S(1)}, u32[]{:S(2)}) copy-start(bf16[8,2,128,256]{3,2,1,0:T(8,128)(2,1)S(1)} %all-to-all-done.refs_0_) | copy-start | bytes 3145732
  166.8 30.9 %all-to-all-start.1 = ((bf16[8,2,128,256]{3,2,1,0:T(8,128)(2,1)}), bf16[8,2,128,256]{3,2,1,0:T(8,128)(2,1)S(1)}, u32[]{:S(2)}, u32[]{:S(2)}) async-start(bf16[8,2,128,256]{3,2,1,0:T(8,128)(2,1)} %bitcast.9), calls=%async_computation.1 | async-start | bytes 2097152 | tf_op jit(solution)/shard_map/all_to_all | solution.py:259
  197.7 1.0 copy-start.4
where the time goes:
time: 204 us; the launch traced here: 203 us
  Pallas kernels  85.2 us (42%)
  waiting for transfers between devices  75.3 us (37%)
  starting transfers between devices  31.6 us (15%)
  local copies, waits for them, and re-layouts  6.06 us (3%)
  other arithmetic  4.27 us (2%)
    pallas_call x2, Pallas kernels, order(): pl.pallas_call(order_kernel, out_shape=jax.ShapeDtypeStruct((len(blocks),...  67.1 us
    ppermute x18, waiting for transfers between devices, along_tp(): return lax.ppermute(array, 'tp', [(n, n ^ hop) for n in range(tp)])  49.5 us
    all_to_all x2, waiting for transfers between devices, body(): lax.all_to_all(by_sequence, 'sp', split_axis=0, concat_axis=0, tiled=True)  25.8 us
    ppermute x18, starting transfers between devices, along_tp(): return lax.ppermute(array, 'tp', [(n, n ^ hop) for n in range(tp)])  21.8 us
    pallas_call x2, Pallas kernels, project(): pl.pallas_call(functools.partial(project_kernel, tp=tp, seqs=seqs, relays...  13.5 us
    all_to_all x2, starting transfers between devices, body(): lax.all_to_all(by_sequence, 'sp', split_axis=0, concat_axis=0, tiled=True)  9.22 us
    pallas_call x1, Pallas kernels, read_cache(): pl.pallas_call(read_kernel, out_shape=[cache, cache, jax.ShapeDtypeStruct...  4.63 us
    unnamed x48, local copies, waits for them, and re-layouts  4.51 us
  transfers between devices with their start and end apart: 21, of which 13 were waited for; matrix products, arithmetic and copies ran while one was open for 1% of the time, Pallas kernels for 20%

commit v1 on v0

--- a/solution.py
+++ b/solution.py
@@ -96,7 +96,7 @@
         order_kernel,
         out_shape=jax.ShapeDtypeStruct((len(blocks),) + blocks[0].shape, blocks[0].dtype),
         in_specs=[pl.BlockSpec(memory_space=pltpu.SMEM)] + [anywhere] * len(blocks),
-        out_specs=anywhere,
+        out_specs=pl.BlockSpec(memory_space=pltpu.VMEM),
         scratch_shapes=[pltpu.SemaphoreType.DMA((len(blocks),))],
         name="order",
     )(place, *blocks)
@@ -216,6 +216,7 @@
         return lax.ppermute(array, "tp", [(n, n ^ hop) for n in range(tp)])
 
     weight = jnp.where(core == 0, key_weight, value_weight)
+    weight, prompt = lax.optimization_barrier((weight, prompt))
     gathered = []
     for chunk in range(chunks):
         part = weight[chunk * step : (chunk + 1) * step]
@@ -254,7 +255,8 @@
         low, own, _ = lax.optimization_barrier((blocks[0], normed, ordered))
         blocks = [low] + blocks[1:]
         outs = project(blocks, relays, own, other, place, key_gain[:, None], tp)
-        ordered = order([outs[0]] + [along_tp(outs[hop], hop) for hop in range(1, tp)], place)
+        sent = [outs[0]] + [along_tp(outs[hop], hop) for hop in range(1, tp)]
+        ordered = order(sent, place)
         by_sequence = ordered.reshape((sp,) + ordered.shape[2:])
         pieces.append(lax.all_to_all(by_sequence, "sp", split_axis=0, concat_axis=0, tiled=True))
 

time: 204 us -> 140 us (0.69)
  Pallas kernels: 85.2 us -> 23.8 us
    pallas_call x2, Pallas kernels: 67.1 us -> 5.71 us  [order(): pl.pallas_call(order_kernel, out_shape=jax.ShapeDtypeStruct((len(blocks),...]
    unnamed x48 -> x50, local copies, waits for them, and re-layouts: 4.51 us -> 4.5 us
  transfers between devices with their start and end apart: 21 -> 21, of which waited for: 13 -> 13; matrix products, arithmetic and copies ran while one was open for 1% -> 2% of each run, Pallas kernels for 20% -> 7%
where the time goes in v1:
time: 140 us
  waiting for transfers between devices  74.9 us (54%)
  starting transfers between devices  31 us (22%)
  Pallas kernels  23.8 us (17%)
  local copies, waits for them, and re-layouts  6.04 us (4%)
  other arithmetic  3.13 us (2%)
    ppermute x18, waiting for transfers between devices, along_tp(): return lax.ppermute(array, 'tp', [(n, n ^ hop) for n in range(tp)])  49.1 us
    all_to_all x2, waiting for transfers between devices, body(): lax.all_to_all(by_sequence, 'sp', split_axis=0, concat_axis=0, tiled=True)  25.8 us
    ppermute x18, starting transfers between devices, along_tp(): return lax.ppermute(array, 'tp', [(n, n ^ hop) for n in range(tp)])  21.2 us
    pallas_call x2, Pallas kernels, project(): pl.pallas_call(functools.partial(project_kernel, tp=tp, seqs=seqs, relays...  13.5 us
    all_to_all x2, starting transfers between devices, body(): lax.all_to_all(by_sequence, 'sp', split_axis=0, concat_axis=0, tiled=True)  9.22 us
    pallas_call x2, Pallas kernels, order(): pl.pallas_call(order_kernel, out_shape=jax.ShapeDtypeStruct((len(blocks),...  5.71 us
    pallas_call x1, Pallas kernels, read_cache(): pl.pallas_call(read_kernel, out_shape=[cache, cache, jax.ShapeDtypeStruct...  4.64 us
    unnamed x50, local copies, waits for them, and re-layouts  4.5 us
  transfers between devices with their start and end apart: 21, of which 13 were waited for; matrix products, arithmetic and copies ran while one was open for 2% of the time, Pallas kernels for 7%

profile of v1, /device:TPU:0, one launch (start us, length us, event | category | flops | bytes accessed | tf_op | source)
XLA Modules:
  0.0 139.8 jit_solution(10582393647365366222)
XLA Ops:
  0.7 1.5 %broadcast_select_fusion = bf16[256,2048]{1,0:T(8,128)(2,1)S(1)} fusion(bf16[256,2048]{1,0:T(8,128)(2,1)} %param.9, bf16[256,2048]{1,0:T(8,128)(2,1)} %param.10, pred[]{:T(512)S(6)} %eq.5), kind=kLoop, calls=%fused_computation.5 | loop fusion | flops 524288 | bytes 3145729 | tf_op jit(solution)/shard_map/jit(_where)/select_n | solution.py:218
  2.6 0.5 fusion
  3.2 0.5 fusion.2.refs_8_
  3.8 0.6 collective-permute-start.6
  4.5 2.6 %collective-permute-start.2 = (bf16[64,2048]{1,0:T(8,128)(2,1)S(1)}, bf16[64,2048]{1,0:T(8,128)(2,1)S(1)}, u32[]{:S(2)}, u32[]{:S(2)}) collective-permute-start(bf16[64,2048]{1,0:T(8,128)(2,1)S(1)} %get-tuple-element.24.refs_0_), channel_id=1, source_target_pairs={{0,2},{1,3},{2,0},{3,1},{4,6},{5,7},{6,4},{7,5},{8,10},{9,11},{10,... | collective-permute-start | bytes 786440 | tf_op jit(solution)/shard_map/ppermute | solution.py:216
  7.1 1.5 %collective-permute-start.1 = (bf16[64,2048]{1,0:T(8,128)(2,1)S(1)}, bf16[64,2048]{1,0:T(8,128)(2,1)}, u32[]{:S(2)}, u32[]{:S(2)}) collective-permute-start(bf16[64,2048]{1,0:T(8,128)(2,1)S(1)} %get-tuple-element.43.refs_1_), channel_id=1, source_target_pairs={{0,1},{1,0},{2,3},{3,2},{4,5},{5,4},{6,7},{7,6},{8,9},{9,8},{10,11... | collective-permute-start | bytes 786440 | tf_op jit(solution)/shard_map/ppermute | solution.py:216
  8.6 0.5 collective-permute-start
  9.2 5.0 %collective-permute-done.2.refs_4_ = bf16[64,2048]{1,0:T(8,128)(2,1)S(1)} collective-permute-done((bf16[64,2048]{1,0:T(8,128)(2,1)S(1)}, bf16[64,2048]{1,0:T(8,128)(2,1)S(1)}, u32[]{:S(2)}, u32[]{:S(2)}) %collective-permute-start.2) | collective-permute-done | bytes 262176 | tf_op jit(solution)/shard_map/ppermute | solution.py:216
  14.2 2.0 %collective-permute-start.4 = (bf16[64,2048]{1,0:T(8,128)(2,1)S(1)}, bf16[64,2048]{1,0:T(8,128)(2,1)}, u32[]{:S(2)}, u32[]{:S(2)}) collective-permute-start(bf16[64,2048]{1,0:T(8,128)(2,1)S(1)} %collective-permute-done.2.refs_4_), channel_id=1, source_target_pairs={{0,1},{1,0},{2,3},{3,2},{4,5},{5,4},{6,7},{7,6},{8,9},{9,8},{10,11... | collective-permute-start | bytes 786440 | tf_op jit(solution)/shard_map/ppermute | solution.py:216
  16.3 1.4 collective-permute-start.5
  17.7 0.7 copy.10.gain
  18.4 0.6 pad_add_fusion.place
  19.0 2.9 %collective-permute-done.refs_2_ = bf16[64,2048]{1,0:T(8,128)(2,1)} collective-permute-done((bf16[64,2048]{1,0:T(8,128)(2,1)S(1)}, bf16[64,2048]{1,0:T(8,128)(2,1)}, u32[]{:S(2)}, u32[]{:S(2)}) %collective-permute-start) | collective-permute-done | bytes 262176 | tf_op jit(solution)/shard_map/ppermute | solution.py:216
  22.0 4.9 %collective-permute-done.4.refs_6_ = bf16[64,2048]{1,0:T(8,128)(2,1)} collective-permute-done((bf16[64,2048]{1,0:T(8,128)(2,1)S(1)}, bf16[64,2048]{1,0:T(8,128)(2,1)}, u32[]{:S(2)}, u32[]{:S(2)}) %collective-permute-start.4) | collective-permute-done | bytes 262176 | tf_op jit(solution)/shard_map/ppermute | solution.py:216
  26.9 6.7 %project.2 = (bf16[2,2,128,256]{3,2,1,0:T(8,128)(2,1)}, bf16[2,2,128,256]{3,2,1,0:T(8,128)(2,1)}, bf16[2,2,128,256]{3,2,1,0:T(8,128)(2,1)}, bf16[2,2,128,256]{3,2,1,0:T(8,128)(2,1)}) custom-call(s32[5]{0:T(128)} %pad_add_fusion.place, f32[64,1]{1,0:T(8,128)} %copy.10.gain, bf16[64,2048]{1,0:T(8,128)(2,1)} %copy-done.9, bf16[64,2048]{1,0:T(8,128)(2,1)} %copy-done.8, ...), custom_call_target="tpu_custom_call" | custom-call | tf_op jit(solution)/shard_map/project/pallas_call | solution.py:63
  33.6 1.6 %collective-permute-start.7 = (bf16[2,2,128,256]{3,2,1,0:T(8,128)(2,1)}, bf16[2,2,128,256]{3,2,1,0:T(8,128)(2,1)S(1)}, u32[]{:S(2)}, u32[]{:S(2)}) collective-permute-start(bf16[2,2,128,256]{3,2,1,0:T(8,128)(2,1)} %get-tuple-element.27), channel_id=1, source_target_pairs={{0,1},{1,0},{2,3},{3,2},{4,5},{5,4},{6,7},{7,6},{8,9},{9,8},{10,11... | collective-permute-start | bytes 786440 | tf_op jit(solution)/shard_map/ppermute | solution.py:216
  35.2 0.5 collective-permute-start.8
  35.7 1.5 %collective-permute-start.9 = (bf16[2,2,128,256]{3,2,1,0:T(8,128)(2,1)}, bf16[2,2,128,256]{3,2,1,0:T(8,128)(2,1)S(1)}, u32[]{:S(2)}, u32[]{:S(2)}) collective-permute-start(bf16[2,2,128,256]{3,2,1,0:T(8,128)(2,1)} %get-tuple-element.29), channel_id=1, source_target_pairs={{0,3},{1,2},{2,1},{3,0},{4,7},{5,6},{6,5},{7,4},{8,11},{9,10},{10,... | collective-permute-start | bytes 786440 | tf_op jit(solution)/shard_map/ppermute | solution.py:216
  37.2 5.9 %collective-permute-done.7.refs_1_ = bf16[2,2,128,256]{3,2,1,0:T(8,128)(2,1)S(1)} collective-permute-done((bf16[2,2,128,256]{3,2,1,0:T(8,128)(2,1)}, bf16[2,2,128,256]{3,2,1,0:T(8,128)(2,1)S(1)}, u32[]{:S(2)}, u32[]{:S(2)}) %collective-permute-start.7) | collective-permute-done | bytes 262176 | tf_op jit(solution)/shard_map/ppermute | solution.py:216
  43.1 5.2 %collective-permute-done.8.refs_2_ = bf16[2,2,128,256]{3,2,1,0:T(8,128)(2,1)S(1)} collective-permute-done((bf16[2,2,128,256]{3,2,1,0:T(8,128)(2,1)}, bf16[2,2,128,256]{3,2,1,0:T(8,128)(2,1)S(1)}, u32[]{:S(2)}, u32[]{:S(2)}) %collective-permute-start.8) | collective-permute-done | bytes 262176 | tf_op jit(solution)/shard_map/ppermute | solution.py:216
  48.3 0.7 copy-done.20
  49.1 2.9 %order.2 = bf16[4,2,2,128,256]{4,3,2,1,0:T(8,128)(2,1)} custom-call(s32[5]{0:T(128)} %pad_add_fusion.place, bf16[2,2,128,256]{3,2,1,0:T(8,128)(2,1)} %get-tuple-element.26.refs_0_, bf16[2,2,128,256]{3,2,1,0:T(8,128)(2,1)} %copy-done.18, bf16[2,2,128,256]{3,2,1,0:T(8,128)(2,1)} %copy-done.20, bf16[2,2,128,256]{3,2,1,0:T(8,128)(2,1)} %copy-done.22), custom_call_target="tpu_custom_call" | custom-call | tf_op jit(solution)/shard_map/order/pallas_call | solution.py:95
  52.0 4.9 %all-to-all-start = ((bf16[8,2,128,256]{3,2,1,0:T(8,128)(2,1)}), bf16[8,2,128,256]{3,2,1,0:T(8,128)(2,1)S(1)}, u32[]{:S(2)}, u32[]{:S(2)}) async-start(bf16[8,2,128,256]{3,2,1,0:T(8,128)(2,1)} %bitcast.8), calls=%async_computation | async-start | bytes 2097152 | tf_op jit(solution)/shard_map/all_to_all | solution.py:261
  56.9 0.5 collective-permute-start.12
  57.4 1.1 collective-permute-start.11
  58.5 0.9 collective-permute-start.10
  59.4 1.5 %collective-permute-start.13 = (bf16[64,2048]{1,0:T(8,128)(2,1)S(1)}, bf16[64,2048]{1,0:T(8,128)(2,1)S(1)}, u32[]{:S(2)}, u32[]{:S(2)}) collective-permute-start(bf16[64,2048]{1,0:T(8,128)(2,1)S(1)} %get-tuple-element.32.refs_1_), channel_id=1, source_target_pairs={{0,2},{1,3},{2,0},{3,1},{4,6},{5,7},{6,4},{7,5},{8,10},{9,11},{10,... | collective-permute-start | bytes 786440 | tf_op jit(solution)/shard_map/ppermute | solution.py:216
  60.9 5.1 %collective-permute-done.12.refs_4_ = bf16[64,2048]{1,0:T(8,128)(2,1)S(1)} collective-permute-done((bf16[64,2048]{1,0:T(8,128)(2,1)S(1)}, bf16[64,2048]{1,0:T(8,128)(2,1)S(1)}, u32[]{:S(2)}, u32[]{:S(2)}) %collective-permute-start.12) | collective-permute-done | bytes 262176 | tf_op jit(solution)/shard_map/ppermute | solution.py:216
  66.0 0.5 collective-permute-start.14
  66.6 1.5 %collective-permute-start.15 = (bf16[64,2048]{1,0:T(8,128)(2,1)S(1)}, bf16[64,2048]{1,0:T(8,128)(2,1)S(1)}, u32[]{:S(2)}, u32[]{:S(2)}) collective-permute-start(bf16[64,2048]{1,0:T(8,128)(2,1)S(1)} %collective-permute-done.11.refs_3_), channel_id=1, source_target_pairs={{0,2},{1,3},{2,0},{3,1},{4,6},{5,7},{6,4},{7,5},{8,10},{9,11},{10,... | collective-permute-start | bytes 786440 | tf_op jit(solution)/shard_map/ppermute | solution.py:216
  68.1 4.1 %collective-permute-done.10.refs_2_ = bf16[64,2048]{1,0:T(8,128)(2,1)S(1)} collective-permute-done((bf16[64,2048]{1,0:T(8,128)(2,1)S(1)}, bf16[64,2048]{1,0:T(8,128)(2,1)S(1)}, u32[]{:S(2)}, u32[]{:S(2)}) %collective-permute-start.10) | collective-permute-done | bytes 262176 | tf_op jit(solution)/shard_map/ppermute | solution.py:216
  72.2 4.9 %collective-permute-done.14.refs_6_ = bf16[64,2048]{1,0:T(8,128)(2,1)S(1)} collective-permute-done((bf16[64,2048]{1,0:T(8,128)(2,1)S(1)}, bf16[64,2048]{1,0:T(8,128)(2,1)S(1)}, u32[]{:S(2)}, u32[]{:S(2)}) %collective-permute-start.14) | collective-permute-done | bytes 262176 | tf_op jit(solution)/shard_map/ppermute | solution.py:216
  77.1 0.7 copy-done.15
  77.8 0.7 copy-done.16
  78.5 6.7 %project.3 = (bf16[2,2,128,256]{3,2,1,0:T(8,128)(2,1)}, bf16[2,2,128,256]{3,2,1,0:T(8,128)(2,1)}, bf16[2,2,128,256]{3,2,1,0:T(8,128)(2,1)}, bf16[2,2,128,256]{3,2,1,0:T(8,128)(2,1)}) custom-call(s32[5]{0:T(128)} %pad_add_fusion.place, f32[64,1]{1,0:T(8,128)} %copy.10.gain, bf16[64,2048]{1,0:T(8,128)(2,1)} %copy-done.7, bf16[64,2048]{1,0:T(8,128)(2,1)} %copy-done.6, ...), custom_call_target="tpu_custom_call" | custom-call | tf_op jit(solution)/shard_map/project/pallas_call | solution.py:63
  85.2 1.1 collective-permute-start.16
  86.4 0.9 collective-permute-start.17
  87.3 1.5 %collective-permute-start.18 = (bf16[2,2,128,256]{3,2,1,0:T(8,128)(2,1)}, bf16[2,2,128,256]{3,2,1,0:T(8,128)(2,1)S(1)}, u32[]{:S(2)}, u32[]{:S(2)}) collective-permute-start(bf16[2,2,128,256]{3,2,1,0:T(8,128)(2,1)} %get-tuple-element.37), channel_id=1, source_target_pairs={{0,3},{1,2},{2,1},{3,0},{4,7},{5,6},{6,5},{7,4},{8,11},{9,10},{10,... | collective-permute-start | bytes 786440 | tf_op jit(solution)/shard_map/ppermute | solution.py:216
  88.8 5.9 %collective-permute-done.16.refs_1_ = bf16[2,2,128,256]{3,2,1,0:T(8,128)(2,1)S(1)} collective-permute-done((bf16[2,2,128,256]{3,2,1,0:T(8,128)(2,1)}, bf16[2,2,128,256]{3,2,1,0:T(8,128)(2,1)S(1)}, u32[]{:S(2)}, u32[]{:S(2)}) %collective-permute-start.16) | collective-permute-done | bytes 262176 | tf_op jit(solution)/shard_map/ppermute | solution.py:216
  94.7 0.7 collective-permute-done.17.refs_2_
  95.4 4.3 %collective-permute-done.18.refs_3_ = bf16[2,2,128,256]{3,2,1,0:T(8,128)(2,1)S(1)} collective-permute-done((bf16[2,2,128,256]{3,2,1,0:T(8,128)(2,1)}, bf16[2,2,128,256]{3,2,1,0:T(8,128)(2,1)S(1)}, u32[]{:S(2)}, u32[]{:S(2)}) %collective-permute-start.18) | collective-permute-done | bytes 262176 | tf_op jit(solution)/shard_map/ppermute | solution.py:216
  99.6 0.7 copy-done.21
  100.3 2.9 %order.3 = bf16[4,2,2,128,256]{4,3,2,1,0:T(8,128)(2,1)} custom-call(s32[5]{0:T(128)} %pad_add_fusion.place, bf16[2,2,128,256]{3,2,1,0:T(8,128)(2,1)} %get-tuple-element.34.refs_0_, bf16[2,2,128,256]{3,2,1,0:T(8,128)(2,1)} %copy-done.17, bf16[2,2,128,256]{3,2,1,0:T(8,128)(2,1)} %copy-done.19, bf16[2,2,128,256]{3,2,1,0:T(8,128)(2,1)} %copy-done.21), custom_call_target="tpu_custom_call" | custom-call | tf_op jit(solution)/shard_map/order/pallas_call | solution.py:95
  103.2 4.3 %all-to-all-start.1 = ((bf16[8,2,128,256]{3,2,1,0:T(8,128)(2,1)}), bf16[8,2,128,256]{3,2,1,0:T(8,128)(2,1)S(1)}, u32[]{:S(2)}, u32[]{:S(2)}) async-start(bf16[8,2,128,256]{3,2,1,0:T(8,128)(2,1)} %bitcast.9), calls=%async_computation.1 | async-start | bytes 2097152 | tf_op jit(solution)/shard_map/all_to_all | solution.py:261
  107.6 0.7 reshape.27.bias
  108.3 25.8 %all-to-all-done.1.refs_1_ = bf16[8,2,128,256]{3,2,1,0:T(8,128)(2,1)S(1)} async-done(((bf16[8,2,128,256]{3,2,1,0:T(8,128)(2,1)}), bf16[8,2,128,256]{3,2,1,0:T(8,128)(2,1)S(1)}, u32[]{:S(2)}, u32[]{:S(2)}) %all-to-all-start.1) | async-done | bytes 1048608 | tf_op jit(solution)/shard_map/all_to_all | solution.py:261
  134.1 1.0 copy-done.5
  135.1 4.6 %read_cache.1 = (bf16[256,2048]{1,0:T(8,128)(2,1)}, bf16[256,2048]{1,0:T(8,128)(2,1)}, bf16[2,256]{1,0:T(2,128)(2,1)}) custom-call(bf16[2,256]{1,0:T(2,128)(2,1)} %bitcast.10, f32[8,1]{1,0:T(8,128)} %reshape.27.bias, bf16[8,2,128,256]{3,2,1,0:T(8,128)(2,1)} %copy-done.4, bf16[8,2,128,256]{3,2,1,0:T(8,128)(2,1)} %copy-done.5), custom_call_target="tpu_custom_call" | custom-call | tf_op jit(solution)/shard_map/read_cache/pallas_call | solution.py:189
  (59 shorter events, 1.1 us)
Async XLA Ops:
  0.6 106.9 %copy-start = (f32[2,16]{1,0:T(2,128)S(1)}, f32[2,16]{1,0:T(2,128)}, u32[]{:S(2)}) copy-start(f32[2,16]{1,0:T(2,128)} %param.13) | copy-start | bytes 388
  0.6 1.9 %copy-start.2 = (bf16[2,256,2048]{2,1,0:T(8,128)(2,1)S(1)}, bf16[2,256,2048]{2,1,0:T(8,128)(2,1)}, u32[]{:S(2)}) copy-start(bf16[2,256,2048]{2,1,0:T(8,128)(2,1)} %param.7) | copy-start | bytes 6291460
  0.7 2.5 %copy-start.3 = (bf16[2,256,2048]{2,1,0:T(8,128)(2,1)S(1)}, bf16[2,256,2048]{2,1,0:T(8,128)(2,1)}, u32[]{:S(2)}) copy-start(bf16[2,256,2048]{2,1,0:T(8,128)(2,1)} %param.7) | copy-start | bytes 6291460
  0.7 2.5 %copy-start.23 = (f32[2048]{0:T(1024)S(1)}, f32[2048]{0:T(1024)}, u32[]{:S(2)}) copy-start(f32[2048]{0:T(1024)} %param.8) | copy-start | bytes 24580
  3.7 23.1 %copy-start.1 = (bf16[2,256,2048]{2,1,0:T(8,128)(2,1)}, bf16[2,256,2048]{2,1,0:T(8,128)(2,1)S(1)}, u32[]{:S(2)}) copy-start(bf16[2,256,2048]{2,1,0:T(8,128)(2,1)S(1)} %fusion.2.refs_8_) | copy-start | bytes 6291460
  3.8 14.0 %copy-start.24 = (f32[64]{0:T(128)S(1)}, f32[64]{0:T(128)}, u32[]{:S(2)}) copy-start(f32[64]{0:T(128)} %param.11) | copy-start | bytes 772
  3.8 23.1 %collective-permute-start.6 = (bf16[2,256,2048]{2,1,0:T(8,128)(2,1)S(1)}, bf16[2,256,2048]{2,1,0:T(8,128)(2,1)}, u32[]{:S(2)}, u32[]{:S(2)}) collective-permute-start(bf16[2,256,2048]{2,1,0:T(8,128)(2,1)S(1)} %fusion.2.refs_8_), channel_id=1, source_target_pairs={{0,4},{4,0},{8,12},{12,8},{16,20},{20,16},{24,28},{28,24},{1,5},{5... | collective-permute-start | bytes 6291464 | tf_op jit(solution)/shard_map/ppermute | solution.py:248
  4.4 22.4 %copy-start.8 = (bf16[64,2048]{1,0:T(8,128)(2,1)}, bf16[64,2048]{1,0:T(8,128)(2,1)S(1)}, u32[]{:S(2)}) copy-start(bf16[64,2048]{1,0:T(8,128)(2,1)S(1)} %get-tuple-element.43.refs_1_) | copy-start | bytes 786436
  4.4 22.4 %copy-start.9 = (bf16[64,2048]{1,0:T(8,128)(2,1)}, bf16[64,2048]{1,0:T(8,128)(2,1)S(1)}, u32[]{:S(2)}) copy-start(bf16[64,2048]{1,0:T(8,128)(2,1)S(1)} %get-tuple-element.24.refs_0_) | copy-start | bytes 786436
  4.5 54.0 %copy-start.7 = (bf16[64,2048]{1,0:T(8,128)(2,1)}, bf16[64,2048]{1,0:T(8,128)(2,1)S(1)}, u32[]{:S(2)}) copy-start(bf16[64,2048]{1,0:T(8,128)(2,1)S(1)} %get-tuple-element.31.refs_0_) | copy-start | bytes 786436
  4.5 55.0 %copy-start.6 = (bf16[64,2048]{1,0:T(8,128)(2,1)}, bf16[64,2048]{1,0:T(8,128)(2,1)S(1)}, u32[]{:S(2)}) copy-start(bf16[64,2048]{1,0:T(8,128)(2,1)S(1)} %get-tuple-element.32.refs_1_) | copy-start | bytes 786436
  4.5 9.7 %collective-permute-start.2 = (bf16[64,2048]{1,0:T(8,128)(2,1)S(1)}, bf16[64,2048]{1,0:T(8,128)(2,1)S(1)}, u32[]{:S(2)}, u32[]{:S(2)}) collective-permute-start(bf16[64,2048]{1,0:T(8,128)(2,1)S(1)} %get-tuple-element.24.refs_0_), channel_id=1, source_target_pairs={{0,2},{1,3},{2,0},{3,1},{4,6},{5,7},{6,4},{7,5},{8,10},{9,11},{10,... | collective-permute-start | bytes 786440 | tf_op jit(solution)/shard_map/ppermute | solution.py:216
  7.1 9.3 %collective-permute-start.1 = (bf16[64,2048]{1,0:T(8,128)(2,1)S(1)}, bf16[64,2048]{1,0:T(8,128)(2,1)}, u32[]{:S(2)}, u32[]{:S(2)}) collective-permute-start(bf16[64,2048]{1,0:T(8,128)(2,1)S(1)} %get-tuple-element.43.refs_1_), channel_id=1, source_target_pairs={{0,1},{1,0},{2,3},{3,2},{4,5},{5,4},{6,7},{7,6},{8,9},{9,8},{10,11... | collective-permute-start | bytes 786440 | tf_op jit(solution)/shard_map/ppermute | solution.py:216
  8.6 13.4 %collective-permute-start = (bf16[64,2048]{1,0:T(8,128)(2,1)S(1)}, bf16[64,2048]{1,0:T(8,128)(2,1)}, u32[]{:S(2)}, u32[]{:S(2)}) collective-permute-start(bf16[64,2048]{1,0:T(8,128)(2,1)S(1)} %get-tuple-element.24.refs_0_), channel_id=1, source_target_pairs={{0,1},{1,0},{2,3},{3,2},{4,5},{5,4},{6,7},{7,6},{8,9},{9,8},{10,11... | collective-permute-start | bytes 786440 | tf_op jit(solution)/shard_map/ppermute | solution.py:216
  9.1 12.9 %collective-permute-start.3 = (bf16[64,2048]{1,0:T(8,128)(2,1)S(1)}, bf16[64,2048]{1,0:T(8,128)(2,1)}, u32[]{:S(2)}, u32[]{:S(2)}) collective-permute-start(bf16[64,2048]{1,0:T(8,128)(2,1)S(1)} %get-tuple-element.43.refs_1_), channel_id=1, source_target_pairs={{0,2},{1,3},{2,0},{3,1},{4,6},{5,7},{6,4},{7,5},{8,10},{9,11},{10,... | collective-permute-start | bytes 786440 | tf_op jit(solution)/shard_map/ppermute | solution.py:216
  14.2 12.6 %copy-start.10 = (bf16[64,2048]{1,0:T(8,128)(2,1)}, bf16[64,2048]{1,0:T(8,128)(2,1)S(1)}, u32[]{:S(2)}) copy-start(bf16[64,2048]{1,0:T(8,128)(2,1)S(1)} %collective-permute-done.2.refs_4_) | copy-start | bytes 786436
  14.2 12.6 %collective-permute-start.4 = (bf16[64,2048]{1,0:T(8,128)(2,1)S(1)}, bf16[64,2048]{1,0:T(8,128)(2,1)}, u32[]{:S(2)}, u32[]{:S(2)}) collective-permute-start(bf16[64,2048]{1,0:T(8,128)(2,1)S(1)} %collective-permute-done.2.refs_4_), channel_id=1, source_target_pairs={{0,1},{1,0},{2,3},{3,2},{4,5},{5,4},{6,7},{7,6},{8,9},{9,8},{10,11... | collective-permute-start | bytes 786440 | tf_op jit(solution)/shard_map/ppermute | solution.py:216
  16.3 10.5 %collective-permute-start.5 = (bf16[64,2048]{1,0:T(8,128)(2,1)}, bf16[64,2048]{1,0:T(8,128)(2,1)}, u32[]{:S(2)}, u32[]{:S(2)}) collective-permute-start(bf16[64,2048]{1,0:T(8,128)(2,1)} %collective-permute-done.1.refs_3_), channel_id=1, source_target_pairs={{0,2},{1,3},{2,0},{3,1},{4,6},{5,7},{6,4},{7,5},{8,10},{9,11},{10,... | collective-permute-start | bytes 786440 | tf_op jit(solution)/shard_map/ppermute | solution.py:216
  33.6 9.5 %collective-permute-start.7 = (bf16[2,2,128,256]{3,2,1,0:T(8,128)(2,1)}, bf16[2,2,128,256]{3,2,1,0:T(8,128)(2,1)S(1)}, u32[]{:S(2)}, u32[]{:S(2)}) collective-permute-start(bf16[2,2,128,256]{3,2,1,0:T(8,128)(2,1)} %get-tuple-element.27), channel_id=1, source_target_pairs={{0,1},{1,0},{2,3},{3,2},{4,5},{5,4},{6,7},{7,6},{8,9},{9,8},{10,11... | collective-permute-start | bytes 786440 | tf_op jit(solution)/shard_map/ppermute | solution.py:216
  35.2 13.1 %collective-permute-start.8 = (bf16[2,2,128,256]{3,2,1,0:T(8,128)(2,1)}, bf16[2,2,128,256]{3,2,1,0:T(8,128)(2,1)S(1)}, u32[]{:S(2)}, u32[]{:S(2)}) collective-permute-start(bf16[2,2,128,256]{3,2,1,0:T(8,128)(2,1)} %get-tuple-element.28), channel_id=1, source_target_pairs={{0,2},{1,3},{2,0},{3,1},{4,6},{5,7},{6,4},{7,5},{8,10},{9,11},{10,... | collective-permute-start | bytes 786440 | tf_op jit(solution)/shard_map/ppermute | solution.py:216
  35.7 12.6 %collective-permute-start.9 = (bf16[2,2,128,256]{3,2,1,0:T(8,128)(2,1)}, bf16[2,2,128,256]{3,2,1,0:T(8,128)(2,1)S(1)}, u32[]{:S(2)}, u32[]{:S(2)}) collective-permute-start(bf16[2,2,128,256]{3,2,1,0:T(8,128)(2,1)} %get-tuple-element.29), channel_id=1, source_target_pairs={{0,3},{1,2},{2,1},{3,0},{4,7},{5,6},{6,5},{7,4},{8,11},{9,10},{10,... | collective-permute-start | bytes 786440 | tf_op jit(solution)/shard_map/ppermute | solution.py:216
  43.1 5.2 %copy-start.18 = (bf16[2,2,128,256]{3,2,1,0:T(8,128)(2,1)}, bf16[2,2,128,256]{3,2,1,0:T(8,128)(2,1)S(1)}, u32[]{:S(2)}) copy-start(bf16[2,2,128,256]{3,2,1,0:T(8,128)(2,1)S(1)} %collective-permute-done.7.refs_1_) | copy-start | bytes 786436
  48.3 0.7 copy-start.20
  48.3 0.8 copy-start.22
  52.0 51.2 %all-to-all-start = ((bf16[8,2,128,256]{3,2,1,0:T(8,128)(2,1)}), bf16[8,2,128,256]{3,2,1,0:T(8,128)(2,1)S(1)}, u32[]{:S(2)}, u32[]{:S(2)}) async-start(bf16[8,2,128,256]{3,2,1,0:T(8,128)(2,1)} %bitcast.8), calls=%async_computation | async-start | bytes 2097152 | tf_op jit(solution)/shard_map/all_to_all | solution.py:261
  56.9 9.2 %collective-permute-start.12 = (bf16[64,2048]{1,0:T(8,128)(2,1)S(1)}, bf16[64,2048]{1,0:T(8,128)(2,1)S(1)}, u32[]{:S(2)}, u32[]{:S(2)}) collective-permute-start(bf16[64,2048]{1,0:T(8,128)(2,1)S(1)} %get-tuple-element.31.refs_0_), channel_id=1, source_target_pairs={{0,2},{1,3},{2,0},{3,1},{4,6},{5,7},{6,4},{7,5},{8,10},{9,11},{10,... | collective-permute-start | bytes 786440 | tf_op jit(solution)/shard_map/ppermute | solution.py:216
  57.4 9.2 %collective-permute-start.11 = (bf16[64,2048]{1,0:T(8,128)(2,1)S(1)}, bf16[64,2048]{1,0:T(8,128)(2,1)S(1)}, u32[]{:S(2)}, u32[]{:S(2)}) collective-permute-start(bf16[64,2048]{1,0:T(8,128)(2,1)S(1)} %get-tuple-element.32.refs_1_), channel_id=1, source_target_pairs={{0,1},{1,0},{2,3},{3,2},{4,5},{5,4},{6,7},{7,6},{8,9},{9,8},{10,11... | collective-permute-start | bytes 786440 | tf_op jit(solution)/shard_map/ppermute | solution.py:216
  58.5 13.7 %collective-permute-start.10 = (bf16[64,2048]{1,0:T(8,128)(2,1)S(1)}, bf16[64,2048]{1,0:T(8,128)(2,1)S(1)}, u32[]{:S(2)}, u32[]{:S(2)}) collective-permute-start(bf16[64,2048]{1,0:T(8,128)(2,1)S(1)} %get-tuple-element.31.refs_0_), channel_id=1, source_target_pairs={{0,1},{1,0},{2,3},{3,2},{4,5},{5,4},{6,7},{7,6},{8,9},{9,8},{10,11... | collective-permute-start | bytes 786440 | tf_op jit(solution)/shard_map/ppermute | solution.py:216
  59.4 12.8 %collective-permute-start.13 = (bf16[64,2048]{1,0:T(8,128)(2,1)S(1)}, bf16[64,2048]{1,0:T(8,128)(2,1)S(1)}, u32[]{:S(2)}, u32[]{:S(2)}) collective-permute-start(bf16[64,2048]{1,0:T(8,128)(2,1)S(1)} %get-tuple-element.32.refs_1_), channel_id=1, source_target_pairs={{0,2},{1,3},{2,0},{3,1},{4,6},{5,7},{6,4},{7,5},{8,10},{9,11},{10,... | collective-permute-start | bytes 786440 | tf_op jit(solution)/shard_map/ppermute | solution.py:216
  66.0 11.1 %copy-start.11 = (bf16[64,2048]{1,0:T(8,128)(2,1)}, bf16[64,2048]{1,0:T(8,128)(2,1)S(1)}, u32[]{:S(2)}) copy-start(bf16[64,2048]{1,0:T(8,128)(2,1)S(1)} %collective-permute-done.12.refs_4_) | copy-start | bytes 786436
  66.0 11.0 %collective-permute-start.14 = (bf16[64,2048]{1,0:T(8,128)(2,1)S(1)}, bf16[64,2048]{1,0:T(8,128)(2,1)S(1)}, u32[]{:S(2)}, u32[]{:S(2)}) collective-permute-start(bf16[64,2048]{1,0:T(8,128)(2,1)S(1)} %collective-permute-done.12.refs_4_), channel_id=1, source_target_pairs={{0,1},{1,0},{2,3},{3,2},{4,5},{5,4},{6,7},{7,6},{8,9},{9,8},{10,11... | collective-permute-start | bytes 786440 | tf_op jit(solution)/shard_map/ppermute | solution.py:216
  66.6 10.5 %copy-start.12 = (bf16[64,2048]{1,0:T(8,128)(2,1)}, bf16[64,2048]{1,0:T(8,128)(2,1)S(1)}, u32[]{:S(2)}) copy-start(bf16[64,2048]{1,0:T(8,128)(2,1)S(1)} %collective-permute-done.11.refs_3_) | copy-start | bytes 786436
  66.6 10.5 %collective-permute-start.15 = (bf16[64,2048]{1,0:T(8,128)(2,1)S(1)}, bf16[64,2048]{1,0:T(8,128)(2,1)S(1)}, u32[]{:S(2)}, u32[]{:S(2)}) collective-permute-start(bf16[64,2048]{1,0:T(8,128)(2,1)S(1)} %collective-permute-done.11.refs_3_), channel_id=1, source_target_pairs={{0,2},{1,3},{2,0},{3,1},{4,6},{5,7},{6,4},{7,5},{8,10},{9,11},{10,... | collective-permute-start | bytes 786440 | tf_op jit(solution)/shard_map/ppermute | solution.py:216
  72.2 4.9 %copy-start.13 = (bf16[64,2048]{1,0:T(8,128)(2,1)}, bf16[64,2048]{1,0:T(8,128)(2,1)S(1)}, u32[]{:S(2)}) copy-start(bf16[64,2048]{1,0:T(8,128)(2,1)S(1)} %collective-permute-done.10.refs_2_) | copy-start | bytes 786436
  72.2 4.9 %copy-start.14 = (bf16[64,2048]{1,0:T(8,128)(2,1)}, bf16[64,2048]{1,0:T(8,128)(2,1)S(1)}, u32[]{:S(2)}) copy-start(bf16[64,2048]{1,0:T(8,128)(2,1)S(1)} %collective-permute-done.13.refs_5_) | copy-start | bytes 786436
  77.1 0.7 copy-start.15
  77.8 0.7 copy-start.16
  85.2 9.5 %collective-permute-start.16 = (bf16[2,2,128,256]{3,2,1,0:T(8,128)(2,1)}, bf16[2,2,128,256]{3,2,1,0:T(8,128)(2,1)S(1)}, u32[]{:S(2)}, u32[]{:S(2)}) collective-permute-start(bf16[2,2,128,256]{3,2,1,0:T(8,128)(2,1)} %get-tuple-element.35), channel_id=1, source_target_pairs={{0,1},{1,0},{2,3},{3,2},{4,5},{5,4},{6,7},{7,6},{8,9},{9,8},{10,11... | collective-permute-start | bytes 786440 | tf_op jit(solution)/shard_map/ppermute | solution.py:216
  86.4 9.0 %collective-permute-start.17 = (bf16[2,2,128,256]{3,2,1,0:T(8,128)(2,1)}, bf16[2,2,128,256]{3,2,1,0:T(8,128)(2,1)S(1)}, u32[]{:S(2)}, u32[]{:S(2)}) collective-permute-start(bf16[2,2,128,256]{3,2,1,0:T(8,128)(2,1)} %get-tuple-element.36), channel_id=1, source_target_pairs={{0,2},{1,3},{2,0},{3,1},{4,6},{5,7},{6,4},{7,5},{8,10},{9,11},{10,... | collective-permute-start | bytes 786440 | tf_op jit(solution)/shard_map/ppermute | solution.py:216
  87.3 12.3 %collective-permute-start.18 = (bf16[2,2,128,256]{3,2,1,0:T(8,128)(2,1)}, bf16[2,2,128,256]{3,2,1,0:T(8,128)(2,1)S(1)}, u32[]{:S(2)}, u32[]{:S(2)}) collective-permute-start(bf16[2,2,128,256]{3,2,1,0:T(8,128)(2,1)} %get-tuple-element.37), channel_id=1, source_target_pairs={{0,3},{1,2},{2,1},{3,0},{4,7},{5,6},{6,5},{7,4},{8,11},{9,10},{10,... | collective-permute-start | bytes 786440 | tf_op jit(solution)/shard_map/ppermute | solution.py:216
  94.7 4.9 %copy-start.17 = (bf16[2,2,128,256]{3,2,1,0:T(8,128)(2,1)}, bf16[2,2,128,256]{3,2,1,0:T(8,128)(2,1)S(1)}, u32[]{:S(2)}) copy-start(bf16[2,2,128,256]{3,2,1,0:T(8,128)(2,1)S(1)} %collective-permute-done.16.refs_1_) | copy-start | bytes 786436
  95.4 4.3 %copy-start.19 = (bf16[2,2,128,256]{3,2,1,0:T(8,128)(2,1)}, bf16[2,2,128,256]{3,2,1,0:T(8,128)(2,1)S(1)}, u32[]{:S(2)}) copy-start(bf16[2,2,128,256]{3,2,1,0:T(8,128)(2,1)S(1)} %collective-permute-done.17.refs_2_) | copy-start | bytes 786436
  99.6 0.7 copy-start.21
  103.2 30.9 %copy-start.4 = (bf16[8,2,128,256]{3,2,1,0:T(8,128)(2,1)}, bf16[8,2,128,256]{3,2,1,0:T(8,128)(2,1)S(1)}, u32[]{:S(2)}) copy-start(bf16[8,2,128,256]{3,2,1,0:T(8,128)(2,1)S(1)} %all-to-all-done.refs_0_) | copy-start | bytes 3145732
  103.2 30.9 %all-to-all-start.1 = ((bf16[8,2,128,256]{3,2,1,0:T(8,128)(2,1)}), bf16[8,2,128,256]{3,2,1,0:T(8,128)(2,1)S(1)}, u32[]{:S(2)}, u32[]{:S(2)}) async-start(bf16[8,2,128,256]{3,2,1,0:T(8,128)(2,1)} %bitcast.9), calls=%async_computation.1 | async-start | bytes 2097152 | tf_op jit(solution)/shard_map/all_to_all | solution.py:261
  134.1 1.0 copy-start.5
